TPU v7x, 32 devices: a whole 2x2x4 slice. The times are simulated.
32 devices in a mesh: sp: 8 (over z, x), tp: 4 (over y, core).
Axes of the slice: x: 2, y: 2, z: 4, core: 2. Of those that a mesh axis runs over, the one named last changes fastest.
Arguments:
- resid: bfloat16 [1024, 2048], P('sp'), may hold values from -8 to 8
- a_val: bfloat16 [1024, 1024], P('sp', 'tp'), may hold values from -8 to 8
- a_gate: bfloat16 [1024, 1024], P('sp', 'tp'), may hold values from -6 to 6
- conv_kernel: bfloat16 [31, 1024], P(None, 'tp'), may hold values from -1 to 1
- conv_bias: float32 [1024], P('tp'), may hold values from -3 to 3
- ln_gain: float32 [1024], P('tp'), may hold values from 0.1 to 1.9
- ln_bias: float32 [1024], P('tp'), may hold values from -3 to 3
- w_out: bfloat16 [1024, 2048], P('tp'), may hold values from -0.1875 to 0.1875
- ffn_gain: float32 [2048], replicated, may hold values from 0.1 to 1.9
- routes: int32 [1024, 4], P('sp'), may hold values from 0 to 7, all different within a row; in each aligned block of 128 rows (0 to 127, 128 to 255, ...) at most 128 rows name the same one
- route_weights: float32 [1024, 4], P('sp'), may hold values from 0.15 to 1.2
- exp_gate: bfloat16 [8, 2048, 4096], P('sp', None, 'tp'), may hold values from -0.125 to 0.125
- exp_up: bfloat16 [8, 2048, 4096], P('sp', None, 'tp'), may hold values from -0.125 to 0.125
- exp_down: bfloat16 [8, 4096, 2048], P('sp', None, 'tp'), may hold values from -0.09375 to 0.09375
- sh_gate: bfloat16 [2048, 512], P(None, 'tp'), may hold values from -0.125 to 0.125
- sh_up: bfloat16 [2048, 512], P(None, 'tp'), may hold values from -0.125 to 0.125
- sh_down: bfloat16 [512, 2048], P(None, 'tp'), may hold values from -0.25 to 0.25
Outputs:
- result: bfloat16 [1024, 2048], P('sp', 'tp')
Inputs may be any that keep to these rules, and one draw needn't show every extreme that they name: `routes`: among the 128 rows of one index of sp, each expert is named at most 128 times, a bound that some block reaches; a row names 4 different experts.
All inputs are finite; a program needn't handle non-finite values.
Results may differ from a plain program's by a relative error of at most 0.007.
Values may be sent and summed in bfloat16 or wider, within the bound.
A program may use at most 64 MiB of HBM per device.

v0:
```python
import jax
import jax.numpy as jnp
from jax import lax
from jax.sharding import PartitionSpec as P

LN_EPS = 1e-05
RMS_EPS = 1e-06


def shifted(value, axis, by):
    size = lax.axis_size(axis)
    pairs = [(i, i + by) for i in range(size) if 0 <= i + by < size]
    return lax.ppermute(value, axis, pairs)


def body(
    resid,
    a_val,
    a_gate,
    conv_kernel,
    conv_bias,
    ln_gain,
    ln_bias,
    w_out,
    ffn_gain,
    routes,
    route_weights,
    exp_gate,
    exp_up,
    exp_down,
    sh_gate,
    sh_up,
    sh_down,
):
    tp_count = lax.axis_size("tp")
    tp_place = lax.axis_index("tp")
    sp_count = lax.axis_size("sp")
    tok_rows = resid.shape[0]
    model_width = resid.shape[1]
    col_width = model_width // tp_count
    col_start = tp_place * col_width
    conv_span = conv_kernel.shape[0]
    channels_all = a_val.shape[1] * tp_count
    gated_in = (a_val.astype(jnp.float32) * jax.nn.sigmoid(a_gate.astype(jnp.float32))).astype(
        jnp.bfloat16
    )
    before = shifted(gated_in[tok_rows - (conv_span - 1) :], "sp", 1)
    padded = jnp.concatenate([before, gated_in], axis=0).astype(jnp.float32)
    kernel = conv_kernel.astype(jnp.float32)

    def add_tap(offset, running):
        window_rows = lax.dynamic_slice_in_dim(padded, offset, tok_rows, 0)
        return running + lax.dynamic_slice_in_dim(kernel, offset, 1, 0) * window_rows

    start_sum = jnp.broadcast_to(conv_bias[None, :], gated_in.shape)
    conv_out = lax.fori_loop(0, conv_span, add_tap, start_sum)
    row_sums = lax.psum((jnp.sum(conv_out, axis=1), jnp.sum(conv_out * conv_out, axis=1)), "tp")
    channel_mean = row_sums[0] / channels_all
    channel_var = row_sums[1] / channels_all - channel_mean * channel_mean
    scaled = (conv_out - channel_mean[:, None]) * lax.rsqrt(
        channel_var[:, None] + LN_EPS
    ) * ln_gain[None, :] + ln_bias[None, :]
    mixed_out = jax.nn.silu(scaled).astype(jnp.bfloat16)
    partial_proj = jnp.dot(mixed_out, w_out, preferred_element_type=jnp.float32)
    projected = lax.psum(partial_proj, "tp")
    middle = (resid.astype(jnp.float32) + projected).astype(jnp.bfloat16)
    middle_f = middle.astype(jnp.float32)
    inverse = lax.rsqrt(jnp.mean(middle_f * middle_f, axis=1, keepdims=True) + RMS_EPS)
    normed = (middle_f * inverse * ffn_gain[None, :]).astype(jnp.bfloat16)
    middle_cols = lax.dynamic_slice_in_dim(middle, col_start, col_width, 1)
    shared_gate = jnp.dot(normed, sh_gate, preferred_element_type=jnp.float32)
    shared_up = jnp.dot(normed, sh_up, preferred_element_type=jnp.float32)
    shared_hidden = (jax.nn.silu(shared_gate) * shared_up).astype(jnp.bfloat16)
    weight_rows = sh_down
    shared = jnp.dot(
        lax.all_gather(shared_hidden, "tp", axis=1, tiled=True),
        weight_rows,
        preferred_element_type=jnp.float32,
    )
    top_count = routes.shape[1]
    local_experts = exp_gate.shape[0]
    experts_all = local_experts * sp_count
    capacity = max(2 * tok_rows * top_count // experts_all, tp_count)
    pair_count = tok_rows * top_count
    chosen = routes.reshape(pair_count)
    one_hot = (chosen[:, None] == jnp.arange(experts_all, dtype=jnp.int32)[None, :]).astype(
        jnp.int32
    )
    earlier = jnp.cumsum(one_hot, axis=0) - one_hot
    place_in = jnp.sum(earlier * one_hot, axis=1)
    slot_of = chosen * capacity + place_in
    owner_ids = (
        jnp.zeros((experts_all * capacity,), jnp.int32)
        .at[slot_of]
        .set(jnp.arange(pair_count, dtype=jnp.int32) + 1)
    )
    owner_grid = owner_ids.reshape(sp_count, local_experts, capacity)
    part_slots = capacity // tp_count
    own_owners = lax.dynamic_slice_in_dim(owner_grid, tp_place * part_slots, part_slots, 2)
    source_row = jnp.maximum(own_owners - 1, 0) // top_count
    taken = normed[source_row.reshape(-1)].reshape(own_owners.shape + (model_width,))
    landed = lax.all_to_all(
        jnp.where((own_owners > 0)[..., None], taken, jnp.zeros((), jnp.bfloat16)),
        "sp",
        split_axis=0,
        concat_axis=0,
        tiled=True,
    )
    arrived = lax.all_gather(landed, "tp", axis=2, tiled=True)
    gate_part = jnp.einsum("sxcd,xdf->sxcf", arrived, exp_gate, preferred_element_type=jnp.float32)
    up_part = jnp.einsum("sxcd,xdf->sxcf", arrived, exp_up, preferred_element_type=jnp.float32)
    expert_hidden = (jax.nn.silu(gate_part) * up_part).astype(jnp.bfloat16)
    weight_rows = exp_down
    expert_sum = jnp.einsum(
        "sxcf,xfd->sxcd",
        lax.all_gather(expert_hidden, "tp", axis=3, tiled=True),
        weight_rows,
        preferred_element_type=jnp.float32,
    )
    expert_out = expert_sum.astype(jnp.bfloat16)
    returned = lax.all_to_all(expert_out, "sp", split_axis=0, concat_axis=0, tiled=True)
    flat_out = returned.reshape(experts_all * capacity, col_width)
    picked = flat_out[slot_of].astype(jnp.float32).reshape(tok_rows, top_count, col_width)
    routed = jnp.sum(picked * route_weights[:, :, None], axis=1)
    return (middle_cols.astype(jnp.float32) + shared + routed).astype(jnp.bfloat16)


def solution(mesh):
    in_specs = (
        P("sp", None),
        P("sp", "tp"),
        P("sp", "tp"),
        P(None, "tp"),
        P("tp"),
        P("tp"),
        P("tp"),
        P("tp", None),
        P(),
        P("sp", None),
        P("sp", None),
        P("sp", None, "tp"),
        P("sp", None, "tp"),
        P("sp", None, "tp"),
        P(None, "tp"),
        P(None, "tp"),
        P(None, "tp"),
    )
    out_specs = P("sp", "tp")
    return jax.shard_map(body, mesh=mesh, in_specs=in_specs, out_specs=out_specs, check_vma=False)
```

profile of v0, /device:TPU:0, one launch (start us, length us, event | category | flops | bytes accessed | tf_op | source)
XLA Modules:
  0.0 262.0 jit_solution(12313480295030517520)
XLA Ops:
  6.5 1.0 multiply_convert_fusion.1
  7.6 4.9 %collective-permute-start = (bf16[30,256]{1,0:T(8,128)(2,1)S(1)}, bf16[30,256]{1,0:T(8,128)(2,1)S(1)}, u32[]{:S(2)}, u32[]{:S(2)}) collective-permute-start(bf16[30,256]{1,0:T(8,128)(2,1)S(1)} %slice.16), channel_id=1, source_target_pairs={{0,4},{4,8},{8,12},{12,16},{16,20},{20,24},{24,28},{1,5},{5,9},{9,... | collective-permute-start | bytes 46088 | tf_op jit(solution)/shard_map/ppermute | solution.py:13
  14.4 1.1 reduce-window.6
  16.7 2.4 scatter_custom_fusion
  19.8 2.4 while.13
  22.4 6.3 %all-reduce = (f32[128]{0:T(128)S(1)}, f32[128]{0:T(128)S(1)}) all-reduce(f32[128]{0:T(128)S(1)} %get-tuple-element.86, f32[128]{0:T(128)S(1)} %get-tuple-element.85), channel_id=1, replica_groups=mesh['sp'=8,'tp'=4] {'tp'}, use_global_device_ids=true, to_apply=%region_5.0 | all-reduce | flops 256 | bytes 2048 | tf_op jit(solution)/shard_map/psum | solution.py:57
  28.7 2.1 fusion.33
  31.2 36.0 %all-reduce.3.cloned.1.call-done = f32[128,2048]{1,0:T(8,128)} async-done(((f32[128,2048]{1,0:T(8,128)}), f32[128,2048]{1,0:T(8,128)}) %all-reduce.3.cloned.1.call-update) | async-done | bytes 1048592 | tf_op jit(solution)/shard_map/psum | solution.py:65
  67.2 1.5 fusion.30
  68.9 1.4 gather_fusion
  70.4 30.6 %all_to_all.10 = bf16[8,1,32,2048]{3,2,1,0:T(8,128)(2,1)} all-to-all(bf16[8,1,32,2048]{3,2,1,0:T(8,128)(2,1)S(1)} %broadcast_select_fusion), channel_id=1, replica_groups=mesh['sp'=8,'tp'=4] {'sp'}, dimensions={0} | all-to-all | bytes 2097152 | tf_op jit(solution)/shard_map/all_to_all | solution.py:102
  101.1 33.4 %all-gather.3.cloned.1.call-done = bf16[8,1,128,2048]{3,2,0,1:T(8,128)(2,1)} async-done(((bf16[8,1,32,2048]{3,2,0,1:T(8,128)(2,1)}), bf16[8,1,128,2048]{3,2,0,1:T(8,128)(2,1)}) %all-gather.3.cloned.1.call-update) | async-done | bytes 4194320 | tf_op jit(solution)/shard_map/all_gather | solution.py:109
  134.6 7.7 %fusion.4 = f32[8,128,1024]{2,1,0:T(8,128)S(1)} fusion(bf16[1,2048,1024]{2,1,0:T(8,128)(2,1)} %param.31, bf16[8,1,128,2048]{3,2,0,1:T(8,128)(2,1)} %all-gather.3.cloned.1.call-done), kind=kOutput, calls=%fused_computation.10 | convolution fusion | flops 4294967296 | bytes 12582912 | tf_op jit(solution)/shard_map/sxcd,xdf->sxcf/dot_general | solution.py:111
  142.2 6.4 %fusion.2 = bf16[8,1,128,1024]{3,2,0,1:T(8,128)(2,1)} fusion(f32[8,128,1024]{2,1,0:T(8,128)S(1)} %fusion.4, bf16[1,2048,1024]{2,1,0:T(8,128)(2,1)S(1)} %copy-done.4, bf16[8,1,128,2048]{3,2,0,1:T(8,128)(2,1)S(1)} %copy-done.5), kind=kOutput, calls=%fused_computation.8 | convolution fusion | flops 4301258752 | bytes 14680064 | tf_op jit(solution)/shard_map/sxcd,xdf->sxcf/dot_general | solution.py:110
  148.6 58.4 %all-gather.5.cloned.1.call-done = bf16[8,1,128,4096]{3,2,0,1:T(8,128)(2,1)} async-done(((bf16[8,1,128,1024]{3,2,0,1:T(8,128)(2,1)}), bf16[8,1,128,4096]{3,2,0,1:T(8,128)(2,1)}) %all-gather.5.cloned.1.call-update) | async-done | bytes 8388624 | tf_op jit(solution)/shard_map/all_gather | solution.py:116
  207.0 10.1 %fusion.22 = bf16[8,1,128,512]{3,2,1,0:T(8,128)(2,1)} fusion(bf16[1,4096,512]{2,1,0:T(8,128)(2,1)} %param.32, bf16[8,1,128,4096]{3,2,0,1:T(8,128)(2,1)} %all-gather.5.cloned.1.call-done), kind=kOutput, calls=%fused_computation.22 | convolution fusion | flops 4295491584 | bytes 13631488 | tf_op jit(solution)/shard_map/sxcf,xfd->sxcd/dot_general | solution.py:114
  217.2 5.5 %all-to-all-start.1 = ((bf16[8,1,128,512]{3,2,1,0:T(8,128)(2,1)}), bf16[8,1,128,512]{3,2,1,0:T(8,128)(2,1)S(1)}, u32[]{:S(2)}, u32[]{:S(2)}) async-start(bf16[8,1,128,512]{3,2,1,0:T(8,128)(2,1)} %fusion.22), calls=%async_computation.1 | async-start | bytes 2097152 | tf_op jit(solution)/shard_map/all_to_all | solution.py:121
  222.8 1.3 fusion.47
  224.1 1.3 fusion.29
  225.5 5.4 %all_gather.9 = bf16[128,512]{1,0:T(8,128)(2,1)S(1)} all-gather(bf16[128,128]{1,0:T(8,128)(2,1)S(1)} %fusion.29), channel_id=1, replica_groups=mesh['sp'=8,'tp'=4] {'tp'}, dimensions={1}, use_global_device_ids=true | all-gather | bytes 163840 | tf_op jit(solution)/shard_map/all_gather | solution.py:76
  230.9 17.9 %all-to-all-done.1 = bf16[8,1,128,512]{3,2,1,0:T(8,128)(2,1)S(1)} async-done(((bf16[8,1,128,512]{3,2,1,0:T(8,128)(2,1)}), bf16[8,1,128,512]{3,2,1,0:T(8,128)(2,1)S(1)}, u32[]{:S(2)}, u32[]{:S(2)}) %all-to-all-start.1) | async-done | bytes 1048608 | tf_op jit(solution)/shard_map/all_to_all | solution.py:121
  248.9 2.6 gather_fusion.1
  251.5 1.4 reshape.152
  253.6 1.9 fusion.28
  (111 shorter events, 6.9 us)
Async XLA Ops:
  6.5 22.2 %copy-start = (bf16[256,2048]{1,0:T(8,128)(2,1)S(1)}, bf16[256,2048]{1,0:T(8,128)(2,1)}, u32[]{:S(2)}) copy-start(bf16[256,2048]{1,0:T(8,128)(2,1)} %param.26) | copy-start | bytes 3145732
  6.5 60.7 %copy-start.1 = (bf16[128,2048]{1,0:T(8,128)(2,1)S(1)}, bf16[128,2048]{1,0:T(8,128)(2,1)}, u32[]{:S(2)}) copy-start(bf16[128,2048]{1,0:T(8,128)(2,1)} %param.19) | copy-start | bytes 1572868
  6.5 60.6 %all-reduce.3.cloned.1.call-start = ((), (), s32[]{:S(2)}) async-start(), calls=%async_computation.2 | async-start | bytes 2097152 | tf_op jit(solution)/shard_map/psum | solution.py:65
  7.6 11.5 %collective-permute-start = (bf16[30,256]{1,0:T(8,128)(2,1)S(1)}, bf16[30,256]{1,0:T(8,128)(2,1)S(1)}, u32[]{:S(2)}, u32[]{:S(2)}) collective-permute-start(bf16[30,256]{1,0:T(8,128)(2,1)S(1)} %slice.16), channel_id=1, source_target_pairs={{0,4},{4,8},{8,12},{12,16},{16,20},{20,24},{24,28},{1,5},{5,9},{9,... | collective-permute-start | bytes 46088 | tf_op jit(solution)/shard_map/ppermute | solution.py:13
  14.2 54.5 %copy-start.2 = (f32[2048]{0:T(1024)S(1)}, f32[2048]{0:T(1024)}, u32[]{:S(2)}) copy-start(f32[2048]{0:T(1024)} %param.27) | copy-start | bytes 24580
  30.9 103.7 %all-gather.3.cloned.1.call-start = ((), (), s32[]{:S(2)}) async-start(), calls=%async_computation.3 | async-start | bytes 5242880 | tf_op jit(solution)/shard_map/all_gather | solution.py:109
  101.1 106.0 %all-gather.5.cloned.1.call-start = ((), (), s32[]{:S(2)}) async-start(), calls=%async_computation.4 | async-start | bytes 10485760 | tf_op jit(solution)/shard_map/all_gather | solution.py:116
  134.5 7.7 %copy-start.4 = (bf16[1,2048,1024]{2,1,0:T(8,128)(2,1)S(1)}, bf16[1,2048,1024]{2,1,0:T(8,128)(2,1)}, u32[]{:S(2)}) copy-start(bf16[1,2048,1024]{2,1,0:T(8,128)(2,1)} %param.30) | copy-start | bytes 12582916
  134.5 7.7 %copy-start.5 = (bf16[8,1,128,2048]{3,2,0,1:T(8,128)(2,1)S(1)}, bf16[8,1,128,2048]{3,2,0,1:T(8,128)(2,1)}, u32[]{:S(2)}) copy-start(bf16[8,1,128,2048]{3,2,0,1:T(8,128)(2,1)} %all-gather.3.cloned.1.call-done) | copy-start | bytes 12582916
  148.6 74.0 %copy-start.3 = (f32[128,4]{0,1:T(4,128)S(1)}, f32[128,4]{0,1:T(4,128)}, u32[]{:S(2)}) copy-start(f32[128,4]{0,1:T(4,128)} %param.29) | copy-start | bytes 6148
  217.2 31.7 %all-to-all-start.1 = ((bf16[8,1,128,512]{3,2,1,0:T(8,128)(2,1)}), bf16[8,1,128,512]{3,2,1,0:T(8,128)(2,1)S(1)}, u32[]{:S(2)}, u32[]{:S(2)}) async-start(bf16[8,1,128,512]{3,2,1,0:T(8,128)(2,1)} %fusion.22), calls=%async_computation.1 | async-start | bytes 2097152 | tf_op jit(solution)/shard_map/all_to_all | solution.py:121
Sparse Core Ops, SparseCore 0:
  31.0 36.1 all-reduce.2
  101.2 33.3 all-gather.2
  148.7 58.2 all-gather.4
where the time goes:
time: 263 us; the launch traced here: 262 us
  waiting for transfers between devices  146 us (56%)
  blocking collectives  42.4 us (16%)
  matrix products  30.9 us (12%)
  between operations  13.3 us (5%)
  starting transfers between devices  10.5 us (4%)
  local copies, waits for them, and re-layouts  10.4 us (4%)
  other arithmetic  7.78 us (3%)
    all_gather x1, waiting for transfers between devices, body(): lax.all_gather(expert_hidden, 'tp', axis=3, tiled=True)  58.4 us
    psum x1, waiting for transfers between devices, body(): projected = lax.psum(partial_proj, 'tp')  36 us
    all_gather x1, waiting for transfers between devices, body(): arrived = lax.all_gather(landed, 'tp', axis=2, tiled=True)  33.4 us
    all_to_all x1, blocking collectives, body(): lax.all_to_all(jnp.where((own_owners > 0)[..., None], taken, jnp.zeros(()...  30.6 us
    all_to_all x1, waiting for transfers between devices, body(): lax.all_to_all(expert_out, 'sp', split_axis=0, concat_axis=0, tiled=True)  17.9 us
    dot_general x1, matrix products, body(): jnp.einsum('sxcf,xfd->sxcd', lax.all_gather(expert_hidden, 'tp', axis=3,...  10.1 us
    dot_general x1, matrix products, body(): jnp.einsum('sxcd,xdf->sxcf', arrived, exp_up, preferred_element_type=jnp....  7.65 us
    dot_general x1, matrix products, body(): jnp.einsum('sxcd,xdf->sxcf', arrived, exp_gate, preferred_element_type=jn...  6.37 us
  transfers between devices with their start and end apart: 5, of which 4 were waited for; matrix products, arithmetic and copies ran while one was open for 4% of the time, Pallas kernels for 0%

commit v1 on v0

--- a/solution.py
+++ b/solution.py
@@ -13,7 +13,7 @@
     return lax.ppermute(value, axis, pairs)
 
 
-def body(
+def body_slots(
     resid,
     a_val,
     a_gate,
@@ -125,6 +125,139 @@
     return (middle_cols.astype(jnp.float32) + shared + routed).astype(jnp.bfloat16)
 
 
+def swapped(value, axis, bit):
+    size = lax.axis_size(axis)
+    return lax.ppermute(value, axis, [(i, i ^ bit) for i in range(size)])
+
+
+def body_dense(
+    resid,
+    a_val,
+    a_gate,
+    conv_kernel,
+    conv_bias,
+    ln_gain,
+    ln_bias,
+    w_out,
+    ffn_gain,
+    routes,
+    route_weights,
+    exp_gate,
+    exp_up,
+    exp_down,
+    sh_gate,
+    sh_up,
+    sh_down,
+):
+    tp_count = lax.axis_size("tp")
+    tp_place = lax.axis_index("tp")
+    core = tp_place % 2
+    row = tp_place // 2
+    sp_count = lax.axis_size("sp")
+    tok_rows, model_width = resid.shape
+    col_width = model_width // tp_count
+    half_width = model_width // 2
+    part_hidden = exp_gate.shape[2]
+    conv_span = conv_kernel.shape[0]
+    channels_all = a_val.shape[1] * tp_count
+
+    other_rows = lax.dynamic_slice_in_dim(exp_down[0], (1 - row) * 2 * part_hidden, 2 * part_hidden, 0)
+    swapped_down = swapped(other_rows, "tp", 2)
+
+    gated_in = (a_val.astype(jnp.float32) * jax.nn.sigmoid(a_gate.astype(jnp.float32))).astype(
+        jnp.bfloat16
+    )
+    before = shifted(gated_in[tok_rows - (conv_span - 1) :], "sp", 1)
+    expert_ids = jnp.arange(sp_count, dtype=jnp.int32)
+    weight_mat = jnp.sum(
+        jnp.where(routes[:, :, None] == expert_ids[None, None, :], route_weights[:, :, None], 0.0),
+        axis=1,
+    )
+    weight_all = lax.all_gather(weight_mat, "sp", axis=0, tiled=True)
+    weight_own = lax.dynamic_slice_in_dim(weight_all, lax.axis_index("sp"), 1, 1)
+    padded = jnp.concatenate([before, gated_in], axis=0).astype(jnp.float32)
+    kernel = conv_kernel.astype(jnp.float32)
+    conv_out = jnp.broadcast_to(conv_bias[None, :], gated_in.shape)
+    for tap in range(conv_span):
+        conv_out = conv_out + kernel[tap : tap + 1] * padded[tap : tap + tok_rows]
+    row_sums = lax.psum((jnp.sum(conv_out, axis=1), jnp.sum(conv_out * conv_out, axis=1)), "tp")
+    channel_mean = row_sums[0] / channels_all
+    channel_var = row_sums[1] / channels_all - channel_mean * channel_mean
+    scaled = (conv_out - channel_mean[:, None]) * lax.rsqrt(
+        channel_var[:, None] + LN_EPS
+    ) * ln_gain[None, :] + ln_bias[None, :]
+    mixed_out = jax.nn.silu(scaled).astype(jnp.bfloat16)
+    partial_proj = jnp.dot(mixed_out, w_out, preferred_element_type=jnp.float32)
+    give = lax.dynamic_slice_in_dim(partial_proj, (1 - core) * half_width, half_width, 1)
+    keep = lax.dynamic_slice_in_dim(partial_proj, core * half_width, half_width, 1)
+    chip_sum = keep + swapped(give.astype(jnp.bfloat16), "tp", 1).astype(jnp.float32)
+    chip_sum = chip_sum.astype(jnp.bfloat16)
+    half_sum = chip_sum.astype(jnp.float32) + swapped(chip_sum, "tp", 2).astype(jnp.float32)
+    resid_half = lax.dynamic_slice_in_dim(resid, core * half_width, half_width, 1)
+    mid_half = (resid_half.astype(jnp.float32) + half_sum).astype(jnp.bfloat16)
+    mid_all = lax.all_gather(mid_half, "sp", axis=0, tiled=True)
+    mid_peer = swapped(mid_half, "tp", 1)
+    first = jnp.where(core == 0, mid_half, mid_peer)
+    second = jnp.where(core == 0, mid_peer, mid_half)
+    middle = jnp.concatenate([first, second], axis=1)
+
+    middle_f = middle.astype(jnp.float32)
+    inverse = lax.rsqrt(jnp.mean(middle_f * middle_f, axis=1, keepdims=True) + RMS_EPS)
+    normed = (middle_f * inverse * ffn_gain[None, :]).astype(jnp.bfloat16)
+    middle_cols = lax.dynamic_slice_in_dim(middle, tp_place * col_width, col_width, 1)
+    shared_gate = jnp.dot(normed, sh_gate, preferred_element_type=jnp.float32)
+    shared_up = jnp.dot(normed, sh_up, preferred_element_type=jnp.float32)
+    shared_hidden = (jax.nn.silu(shared_gate) * shared_up).astype(jnp.bfloat16)
+    shared = jnp.dot(
+        lax.all_gather(shared_hidden, "tp", axis=1, tiled=True),
+        sh_down,
+        preferred_element_type=jnp.float32,
+    )
+
+    mid_all_peer = swapped(mid_all, "tp", 1)
+    rows_first = jnp.where(core == 0, mid_all, mid_all_peer)
+    rows_second = jnp.where(core == 0, mid_all_peer, mid_all)
+    rows_f = jnp.concatenate([rows_first, rows_second], axis=1).astype(jnp.float32)
+    rows_inverse = lax.rsqrt(jnp.mean(rows_f * rows_f, axis=1, keepdims=True) + RMS_EPS)
+    rows = (rows_f * rows_inverse * ffn_gain[None, :]).astype(jnp.bfloat16)
+    gate_part = jnp.dot(rows, exp_gate[0], preferred_element_type=jnp.float32)
+    up_part = jnp.dot(rows, exp_up[0], preferred_element_type=jnp.float32)
+    hidden = (jax.nn.silu(gate_part) * up_part).astype(jnp.bfloat16)
+    hidden_peer = swapped(hidden, "tp", 1)
+
+    own_at = tp_place * part_hidden
+    peer_at = (tp_place ^ 1) * part_hidden
+    stay = lax.dynamic_slice_in_dim
+    out_own = jnp.dot(
+        hidden, stay(exp_down[0], own_at, part_hidden, 0), preferred_element_type=jnp.float32
+    ) + jnp.dot(
+        hidden_peer, stay(exp_down[0], peer_at, part_hidden, 0), preferred_element_type=jnp.float32
+    )
+    out_far = jnp.dot(
+        hidden, stay(swapped_down, core * part_hidden, part_hidden, 0), preferred_element_type=jnp.float32
+    ) + jnp.dot(
+        hidden_peer,
+        stay(swapped_down, (1 - core) * part_hidden, part_hidden, 0),
+        preferred_element_type=jnp.float32,
+    )
+    both = jnp.concatenate([out_own * weight_own, out_far * weight_own], axis=1).astype(jnp.bfloat16)
+    summed = lax.psum_scatter(both, "sp", scatter_dimension=0, tiled=True)
+    far = swapped(summed[:, col_width:], "tp", 2)
+    routed = summed[:, :col_width].astype(jnp.float32) + far.astype(jnp.float32)
+    return (middle_cols.astype(jnp.float32) + shared + routed).astype(jnp.bfloat16)
+
+
+def body(*args):
+    tok_rows = args[0].shape[0]
+    top_count = args[9].shape[1]
+    local_experts = args[11].shape[0]
+    experts_all = local_experts * lax.axis_size("sp")
+    capacity = 2 * tok_rows * top_count // experts_all
+    if local_experts == 1 and lax.axis_size("tp") == 4 and capacity >= tok_rows:
+        return body_dense(*args)
+    return body_slots(*args)
+
+
 def solution(mesh):
     in_specs = (
         P("sp", None),

time: 263 us -> 231 us (0.88)
  waiting for transfers between devices: 146 us -> 123 us
  matrix products: 30.9 us -> 25.8 us
  local copies, waits for them, and re-layouts: 10.4 us -> 5.9 us
    reduce_scatter x0 -> x1, waiting for transfers between devices: none -> 58 us  [body_dense(): summed = lax.psum_scatter(both, 'sp', scatter_dimension=0, tiled=True)]
    all_gather x2 -> x1, waiting for transfers between devices: 91.8 us -> 50.1 us  [body_dense(): mid_all = lax.all_gather(mid_half, 'sp', axis=0, tiled=True)]
    psum x1 -> x0, waiting for transfers between devices: 36 us -> none  [body(): projected = lax.psum(partial_proj, 'tp')]
    all_gather x1 -> x2, blocking collectives: 5.45 us -> 36.2 us  [the longest x1 30.8 us: body_dense(): weight_all = lax.all_gather(weight_mat, 'sp', axis=0, tiled=True)]
    all_to_all x1 -> x0, blocking collectives: 30.6 us -> none  [body(): lax.all_to_all(jnp.where((own_owners > 0)[..., None], taken, jnp.zeros(()...]
    all_to_all x1 -> x0, waiting for transfers between devices: 17.9 us -> none  [body(): lax.all_to_all(expert_out, 'sp', split_axis=0, concat_axis=0, tiled=True)]
    ppermute x0 -> x7, waiting for transfers between devices: none -> 14.8 us  [swapped(): return lax.ppermute(value, axis, [(i, i ^ bit) for i in range(size)])]
    all_to_all x1 -> x0, starting transfers between devices: 5.51 us -> none  [body(): lax.all_to_all(expert_out, 'sp', split_axis=0, concat_axis=0, tiled=True)]
  transfers between devices with their start and end apart: 5 -> 10, of which waited for: 4 -> 7; matrix products, arithmetic and copies ran while one was open for 4% -> 10% of each run, Pallas kernels for 0% -> 0%
where the time goes in v1:
time: 231 us
  waiting for transfers between devices  123 us (53%)
  blocking collectives  42.6 us (18%)
  matrix products  25.8 us (11%)
  between operations  13.7 us (6%)
  other arithmetic  10.3 us (4%)
  starting transfers between devices  9.37 us (4%)
  local copies, waits for them, and re-layouts  5.9 us (3%)
    reduce_scatter x1, waiting for transfers between devices, body_dense(): summed = lax.psum_scatter(both, 'sp', scatter_dimension=0, tiled=True)  58 us
    all_gather x1, waiting for transfers between devices, body_dense(): mid_all = lax.all_gather(mid_half, 'sp', axis=0, tiled=True)  50.1 us
    all_gather x1, blocking collectives, body_dense(): weight_all = lax.all_gather(weight_mat, 'sp', axis=0, tiled=True)  30.8 us
    ppermute x7, waiting for transfers between devices, swapped(): return lax.ppermute(value, axis, [(i, i ^ bit) for i in range(size)])  14.8 us
    dot_general x1, matrix products, body_dense(): up_part = jnp.dot(rows, exp_up[0], preferred_element_type=jnp.float32)  6.37 us
    psum x1, blocking collectives, body_dense(): lax.psum((jnp.sum(conv_out, axis=1), jnp.sum(conv_out * conv_out, axis=1)...  6.33 us
    all_gather x1, blocking collectives, body_dense(): lax.all_gather(shared_hidden, 'tp', axis=1, tiled=True)  5.45 us
    ppermute x1, starting transfers between devices, shifted(): return lax.ppermute(value, axis, pairs)  4.87 us
  transfers between devices with their start and end apart: 10, of which 7 were waited for; matrix products, arithmetic and copies ran while one was open for 10% of the time, Pallas kernels for 0%

profile of v1, /device:TPU:0, one launch (start us, length us, event | category | flops | bytes accessed | tf_op | source)
XLA Modules:
  0.0 230.6 jit_solution(7663626764208417222)
XLA Ops:
  7.6 4.9 %collective-permute-start = (bf16[30,256]{1,0:T(8,128)(2,1)S(1)}, bf16[30,256]{1,0:T(8,128)(2,1)S(1)}, u32[]{:S(2)}, u32[]{:S(2)}) collective-permute-start(bf16[30,256]{1,0:T(8,128)(2,1)S(1)} %slice.261), channel_id=1, source_target_pairs={{0,4},{4,8},{8,12},{12,16},{16,20},{20,24},{24,28},{1,5},{5,9},{9,... | collective-permute-start | bytes 46088 | tf_op jit(solution)/shard_map/ppermute | solution.py:13
  14.5 1.3 fusion.71
  15.8 6.3 %all-reduce = (f32[128]{0:T(128)S(1)}, f32[128]{0:T(128)S(1)}) all-reduce(f32[128]{0:T(128)S(1)} %get-tuple-element.6, f32[128]{0:T(128)S(1)} %get-tuple-element.5), channel_id=1, replica_groups=mesh['sp'=8,'tp'=4] {'tp'}, use_global_device_ids=true, to_apply=%region_3.4 | all-reduce | flops 256 | bytes 2048 | tf_op jit(solution)/shard_map/psum | solution.py:183
  22.7 1.5 collective-permute-done.1
  25.4 7.3 %collective-permute-done.2 = bf16[128,1024]{1,0:T(8,128)(2,1)S(1)} collective-permute-done((bf16[128,1024]{1,0:T(8,128)(2,1)S(1)}, bf16[128,1024]{1,0:T(8,128)(2,1)S(1)}, u32[]{:S(2)}, u32[]{:S(2)}) %collective-permute-start.2) | collective-permute-done | bytes 262176 | tf_op jit(solution)/shard_map/ppermute | solution.py:130
  33.6 50.1 %all-gather.2.cloned.1.call-done = bf16[1024,1024]{1,0:T(8,128)(2,1)} async-done(((bf16[128,1024]{1,0:T(8,128)(2,1)}), bf16[1024,1024]{1,0:T(8,128)(2,1)}) %all-gather.2.cloned.1.call-update) | async-done | bytes 2097168 | tf_op jit(solution)/shard_map/all_gather | solution.py:198
  83.8 1.7 dynamic-slice_bitcast_fusion
  85.5 1.5 collective-permute-start.6
  88.3 2.5 %broadcast_select_fusion.1 = (bf16[1024,1024]{1,0:T(8,128)(2,1)S(1)}, bf16[1024,1024]{1,0:T(8,128)(2,1)S(1)}) fusion(bf16[1024,1024]{1,0:T(8,128)(2,1)} %all-gather.2.cloned.1.call-done, bf16[1024,1024]{1,0:T(8,128)(2,1)} %collective-permute-done.4, pred[]{:T(512)S(6)} %eq.10), kind=kLoop, calls=%fused_computation.16 | loop fusion | flops 2097152 | bytes 8388609 | tf_op jit(solution)/shard_map/jit(_where)/select_n | solution.py:218
  92.9 4.6 %fusion.5 = f32[1024,1024]{1,0:T(8,128)S(1)} fusion(bf16[1,2048,1024]{2,1,0:T(8,128)(2,1)S(1)} %copy-done.8, f32[2048]{0:T(1024)S(1)} %copy-done.11, f32[1024]{0:T(1024)S(1)} %add_rsqrt_fusion, bf16[1024,1024]{1,0:T(8,128)(2,1)S(1)} %get-tuple-element.11, bf16[1024,1024]{1,0:T(8,128)(2,1)S(1)} %get-tuple-element.10), kind=kOutput, calls=%fused_computation.8 | convolution fusion | flops 4309647360 | bytes 12595200 | tf_op jit(solution)/shard_map/dot_general | solution.py:223
  97.5 6.4 %multiply_convert_fusion = bf16[1024,1024]{1,0:T(8,128)(2,1)} fusion(f32[1024,1024]{1,0:T(8,128)S(1)} %fusion.5, bf16[1,2048,1024]{2,1,0:T(8,128)(2,1)S(1)} %copy-done.9, f32[2048]{0:T(1024)S(1)} %copy-done.11, f32[1024]{0:T(1024)S(1)} %add_rsqrt_fusion, bf16[1024,1024]{1,0:T(8,128)(2,1)S(1)} %get-tuple-element.11, bf16[1024,1024]{1,0:T(8,128)(2,1)S(1)} %get-tuple-element.10), kind=kOutput, calls=%fused_computation.10 | convolution fusion | flops 4315938816 | bytes 14692352 | tf_op jit(solution)/shard_map/dot_general | solution.py:224
  104.1 30.8 %all_gather.11 = f32[1024,8]{0,1:T(8,128)S(1)} all-gather(f32[128,8]{0,1:T(8,128)S(1)} %select_reduce_fusion), channel_id=1, replica_groups=mesh['sp'=8,'tp'=4] {'sp'}, dimensions={0}, use_global_device_ids=true | all-gather | bytes 36864 | tf_op jit(solution)/shard_map/all_gather | solution.py:176
  134.9 3.1 %fusion.12 = f32[1024,512]{1,0:T(8,128)S(1)} fusion(bf16[1024,1024]{1,0:T(8,128)(2,1)} %multiply_convert_fusion, bf16[1,4096,512]{2,1,0:T(8,128)(2,1)} %param.30, s32[]{:T(128)S(6)} %select_n.73), kind=kOutput, calls=%fused_computation.25 | convolution fusion | flops 1073741824 | bytes 5242884 | tf_op jit(solution)/shard_map/dot_general | solution.py:231
  138.0 3.1 %fusion.14 = f32[1024,512]{1,0:T(8,128)S(1)} fusion(bf16[1024,1024]{1,0:T(8,128)(2,1)} %collective-permute-done.5, bf16[2048,512]{1,0:T(8,128)(2,1)} %collective-permute-done.6, s32[]{:T(128)S(6)} %select_n.66), kind=kOutput, calls=%fused_computation.27 | convolution fusion | flops 1073741824 | bytes 5242884 | tf_op jit(solution)/shard_map/dot_general | solution.py:238
  141.1 3.1 %multiply_convert_fusion.1 = bf16[1024,512]{1,0:T(8,128)(2,1)S(1)} fusion(f32[1024,512]{1,0:T(8,128)S(1)} %fusion.14, bf16[1024,1024]{1,0:T(8,128)(2,1)} %multiply_convert_fusion, bf16[2048,512]{1,0:T(8,128)(2,1)} %collective-permute-done.6, s32[]{:T(128)S(6)} %select_n.65, f32[1024]{0:T(1024)S(1)} %bitcast.88), kind=kOutput, calls=%fused_computation.12 | convolution fusion | flops 1075314688 | bytes 6295556 | tf_op jit(solution)/shard_map/dot_general | solution.py:236
  144.2 3.1 %multiply_convert_fusion.2 = bf16[1024,512]{1,0:T(8,128)(2,1)S(1)} fusion(f32[1024,512]{1,0:T(8,128)S(1)} %fusion.12, bf16[1024,1024]{1,0:T(8,128)(2,1)} %collective-permute-done.5, f32[1024]{0:T(1024)S(1)} %bitcast.89, bf16[1,4096,512]{2,1,0:T(8,128)(2,1)} %param.30, s32[]{:T(128)S(6)} %select_n.74), kind=kOutput, calls=%fused_computation.14 | convolution fusion | flops 1075314688 | bytes 6295556 | tf_op jit(solution)/shard_map/dot_general | solution.py:233
  147.4 1.6 pad_maximum_fusion.1
  149.1 1.5 collective-permute-done.3
  151.2 1.4 fusion.7
  152.6 5.4 %all_gather.9 = bf16[128,512]{1,0:T(8,128)(2,1)S(1)} all-gather(bf16[128,128]{1,0:T(8,128)(2,1)S(1)} %fusion.7), channel_id=1, replica_groups=mesh['sp'=8,'tp'=4] {'tp'}, dimensions={1}, use_global_device_ids=true | all-gather | bytes 163840 | tf_op jit(solution)/shard_map/all_gather | solution.py:212
  158.1 58.0 %reduce-scatter.2.cloned.1.call-done = bf16[128,1024]{1,0:T(8,128)(2,1)} async-done(((bf16[1024,1024]{1,0:T(8,128)(2,1)}), bf16[128,1024]{1,0:T(8,128)(2,1)}) %reduce-scatter.2.cloned.1.call-update) | async-done | bytes 262160 | tf_op jit(solution)/shard_map/reduce_scatter | solution.py:244
  217.0 1.5 collective-permute-start.7
  218.8 3.3 %collective-permute-done.7 = bf16[128,512]{1,0:T(8,128)(2,1)S(1)} collective-permute-done((bf16[128,512]{1,0:T(8,128)(2,1)S(1)}, bf16[128,512]{1,0:T(8,128)(2,1)S(1)}, u32[]{:S(2)}, u32[]{:S(2)}) %collective-permute-start.7) | collective-permute-done | bytes 131104 | tf_op jit(solution)/shard_map/ppermute | solution.py:130
  222.0 1.7 add_convert_fusion.2
  (57 shorter events, 11.0 us)
Async XLA Ops:
  6.5 15.6 %copy-start = (bf16[256,2048]{1,0:T(8,128)(2,1)S(1)}, bf16[256,2048]{1,0:T(8,128)(2,1)}, u32[]{:S(2)}) copy-start(bf16[256,2048]{1,0:T(8,128)(2,1)} %param.24) | copy-start | bytes 3145732
  6.5 15.6 %copy-start.6 = (f32[256]{0:T(256)S(1)}, f32[256]{0:T(256)}, u32[]{:S(2)}) copy-start(f32[256]{0:T(256)} %param.23) | copy-start | bytes 3076
  6.5 15.7 %copy-start.7 = (f32[256]{0:T(256)S(1)}, f32[256]{0:T(256)}, u32[]{:S(2)}) copy-start(f32[256]{0:T(256)} %param.22) | copy-start | bytes 3076
  6.5 77.2 %all-gather.2.cloned.1.call-start = ((), (), s32[]{:S(2)}) async-start(), calls=%async_computation.1 | async-start | bytes 2359296 | tf_op jit(solution)/shard_map/all_gather | solution.py:198
  7.6 6.9 %collective-permute-start = (bf16[30,256]{1,0:T(8,128)(2,1)S(1)}, bf16[30,256]{1,0:T(8,128)(2,1)S(1)}, u32[]{:S(2)}, u32[]{:S(2)}) collective-permute-start(bf16[30,256]{1,0:T(8,128)(2,1)S(1)} %slice.261), channel_id=1, source_target_pairs={{0,4},{4,8},{8,12},{12,16},{16,20},{20,24},{24,28},{1,5},{5,9},{9,... | collective-permute-start | bytes 46088 | tf_op jit(solution)/shard_map/ppermute | solution.py:13
  14.5 18.3 %copy-start.3 = (bf16[128,2048]{1,0:T(8,128)(2,1)S(1)}, bf16[128,2048]{1,0:T(8,128)(2,1)}, u32[]{:S(2)}) copy-start(bf16[128,2048]{1,0:T(8,128)(2,1)} %param.17) | copy-start | bytes 1572868
  22.6 1.6 collective-permute-start.1
  24.3 8.4 %collective-permute-start.2 = (bf16[128,1024]{1,0:T(8,128)(2,1)S(1)}, bf16[128,1024]{1,0:T(8,128)(2,1)S(1)}, u32[]{:S(2)}, u32[]{:S(2)}) collective-permute-start(bf16[128,1024]{1,0:T(8,128)(2,1)S(1)} %add_convert_fusion.1), channel_id=1, source_target_pairs={{0,2},{1,3},{2,0},{3,1},{4,6},{5,7},{6,4},{7,5},{8,10},{9,11},{10,... | collective-permute-start | bytes 786440 | tf_op jit(solution)/shard_map/ppermute | solution.py:130
  33.6 182.5 %reduce-scatter.2.cloned.1.call-start = ((), (), s32[]{:S(2)}) async-start(), calls=%async_computation.2 | async-start | bytes 2359296 | tf_op jit(solution)/shard_map/reduce_scatter | solution.py:244
  83.8 4.5 %collective-permute-start.4 = (bf16[1024,1024]{1,0:T(8,128)(2,1)}, bf16[1024,1024]{1,0:T(8,128)(2,1)}, u32[]{:S(2)}, u32[]{:S(2)}) collective-permute-start(bf16[1024,1024]{1,0:T(8,128)(2,1)} %all-gather.2.cloned.1.call-done), channel_id=1, source_target_pairs={{0,1},{1,0},{2,3},{3,2},{4,5},{5,4},{6,7},{7,6},{8,9},{9,8},{10,11... | collective-permute-start | bytes 6291464 | tf_op jit(solution)/shard_map/ppermute | solution.py:130
  85.5 52.5 %collective-permute-start.6 = (bf16[2048,512]{1,0:T(8,128)(2,1)S(1)}, bf16[2048,512]{1,0:T(8,128)(2,1)}, u32[]{:S(2)}, u32[]{:S(2)}) collective-permute-start(bf16[2048,512]{1,0:T(8,128)(2,1)S(1)} %dynamic-slice_bitcast_fusion), channel_id=1, source_target_pairs={{0,2},{1,3},{2,0},{3,1},{4,6},{5,7},{6,4},{7,5},{8,10},{9,11},{10,... | collective-permute-start | bytes 6291464 | tf_op jit(solution)/shard_map/ppermute | solution.py:130
  90.8 2.2 copy-start.8
  90.8 2.2 copy-start.11
  92.9 4.6 %copy-start.9 = (bf16[1,2048,1024]{2,1,0:T(8,128)(2,1)S(1)}, bf16[1,2048,1024]{2,1,0:T(8,128)(2,1)}, u32[]{:S(2)}) copy-start(bf16[1,2048,1024]{2,1,0:T(8,128)(2,1)} %param.29) | copy-start | bytes 12582916
  97.5 6.5 %copy-start.4 = (f32[128,4]{0,1:T(4,128)S(1)}, f32[128,4]{0,1:T(4,128)}, u32[]{:S(2)}) copy-start(f32[128,4]{0,1:T(4,128)} %param.27) | copy-start | bytes 6148
  97.5 6.5 %copy-start.5 = (s32[128,4]{0,1:T(4,128)S(1)}, s32[128,4]{0,1:T(4,128)}, u32[]{:S(2)}) copy-start(s32[128,4]{0,1:T(4,128)} %param.26) | copy-start | bytes 6148
  103.9 34.1 %collective-permute-start.5 = (bf16[1024,1024]{1,0:T(8,128)(2,1)}, bf16[1024,1024]{1,0:T(8,128)(2,1)}, u32[]{:S(2)}, u32[]{:S(2)}) collective-permute-start(bf16[1024,1024]{1,0:T(8,128)(2,1)} %multiply_convert_fusion), channel_id=1, source_target_pairs={{0,1},{1,0},{2,3},{3,2},{4,5},{5,4},{6,7},{7,6},{8,9},{9,8},{10,11... | collective-permute-start | bytes 6291464 | tf_op jit(solution)/shard_map/ppermute | solution.py:130
  147.4 1.6 copy-start.1
  147.4 3.5 %copy-start.10 = (bf16[2048,128]{1,0:T(8,128)(2,1)S(1)}, bf16[2048,128]{1,0:T(8,128)(2,1)}, u32[]{:S(2)}) copy-start(bf16[2048,128]{1,0:T(8,128)(2,1)} %param.31) | copy-start | bytes 1572868
  149.0 69.6 %copy-start.2 = (bf16[512,512]{1,0:T(8,128)(2,1)S(1)}, bf16[512,512]{1,0:T(8,128)(2,1)}, u32[]{:S(2)}) copy-start(bf16[512,512]{1,0:T(8,128)(2,1)} %param.33) | copy-start | bytes 1572868
  149.0 1.6 collective-permute-start.3
  217.0 5.0 %collective-permute-start.7 = (bf16[128,512]{1,0:T(8,128)(2,1)S(1)}, bf16[128,512]{1,0:T(8,128)(2,1)S(1)}, u32[]{:S(2)}, u32[]{:S(2)}) collective-permute-start(bf16[128,512]{1,0:T(8,128)(2,1)S(1)} %slice.324), channel_id=1, source_target_pairs={{0,2},{1,3},{2,0},{3,1},{4,6},{5,7},{6,4},{7,5},{8,10},{9,11},{10,... | collective-permute-start | bytes 393224 | tf_op jit(solution)/shard_map/ppermute | solution.py:130
Sparse Core Ops, SparseCore 0:
  33.7 50.0 all-gather.1
  149.1 66.9 reduce-scatter.1

commit v2 on v1

--- a/solution.py
+++ b/solution.py
@@ -1,6 +1,10 @@
+import functools
+
 import jax
 import jax.numpy as jnp
 from jax import lax
+from jax.experimental import pallas as pl
+from jax.experimental.pallas import tpu as pltpu
 from jax.sharding import PartitionSpec as P
 
 LN_EPS = 1e-05
@@ -130,6 +134,212 @@
     return lax.ppermute(value, axis, [(i, i ^ bit) for i in range(size)])
 
 
+def gather_kernel(
+    levels,
+    own_ref,
+    weight_ref,
+    down_ref,
+    rows_ref,
+    weights_ref,
+    swap_ref,
+    local_sem,
+    up_sem,
+    low_sem,
+    side_sem,
+    core_sem,
+    main_recv,
+    core_recv,
+    weight_send,
+    weight_recv,
+    swap_sem,
+):
+    count = 2 * levels
+    me = lax.axis_index("sp")
+    tp_place = lax.axis_index("tp")
+    level, side = me // 2, me % 2
+    row, core = tp_place // 2, tp_place % 2
+    core_peer = {"tp": row * 2 + (1 - core)}
+    row_peer = {"tp": (1 - row) * 2 + core}
+    side_peer = {"sp": level * 2 + (1 - side)}
+    mesh_ids = pl.DeviceIdType.MESH
+
+    barrier = pltpu.get_barrier_semaphore()
+    others = [lax.rem(me + step, count) for step in range(1, count)]
+    for other in others:
+        pl.semaphore_signal(barrier, inc=1, device_id={"sp": other}, device_id_type=mesh_ids)
+    pl.semaphore_signal(barrier, inc=1, device_id=core_peer, device_id_type=mesh_ids)
+    pl.semaphore_signal(barrier, inc=1, device_id=row_peer, device_id_type=mesh_ids)
+    pl.semaphore_wait(barrier, count + 1)
+
+    def remote(src, dst, send, recv, where):
+        return pltpu.make_async_remote_copy(
+            src_ref=src, dst_ref=dst, send_sem=send, recv_sem=recv, device_id=where, device_id_type=mesh_ids
+        )
+
+    def block(at):
+        return rows_ref.at[core, at]
+
+    half_rows = swap_ref.shape[0]
+    swap = remote(
+        down_ref.at[0, pl.ds(pl.multiple_of((1 - row) * half_rows, half_rows), half_rows)],
+        swap_ref,
+        swap_sem.at[0],
+        swap_sem.at[1],
+        row_peer,
+    )
+
+    def up_copy(src, origin):
+        at = origin * 2 + side
+        return remote(src, block(at), up_sem.at[origin], main_recv.at[at], {"sp": me + 2})
+
+    def low_copy(src, origin):
+        at = origin * 2 + side
+        return remote(src, block(at), low_sem.at[origin], main_recv.at[at], {"sp": me - 2})
+
+    def side_copy(src, origin):
+        at = origin * 2 + side
+        return remote(src, block(at), side_sem.at[origin], main_recv.at[at], side_peer)
+
+    def core_copy(src, at):
+        return remote(src, block(at), core_sem.at[at], core_recv.at[at], core_peer)
+
+    def landed(at):
+        remote(block(at), block(at), core_sem.at[at], main_recv.at[at], core_peer).wait_recv()
+
+    @pl.when(level < levels - 1)
+    def _():
+        up_copy(own_ref, level).start()
+
+    @pl.when(level > 0)
+    def _():
+        low_copy(own_ref, level).start()
+
+    side_copy(own_ref, level).start()
+    swap.start()
+    core_copy(own_ref, me).start()
+    weight_copies = [
+        remote(
+            weight_ref,
+            weights_ref.at[me],
+            weight_send.at[step],
+            weight_recv.at[me],
+            {"sp": other},
+        )
+        for step, other in enumerate(others)
+    ]
+    for copy in weight_copies:
+        copy.start()
+    keep = pltpu.make_async_copy(own_ref, block(me), local_sem.at[0])
+    keep.start()
+    keep_weight = pltpu.make_async_copy(weight_ref, weights_ref.at[me], local_sem.at[1])
+    keep_weight.start()
+
+    for step in range(1, levels):
+        below = level - step
+        above = level + step
+
+        @pl.when(below >= 0)
+        def _():
+            at = below * 2 + side
+            landed(at)
+
+            @pl.when(level < levels - 1)
+            def _():
+                up_copy(block(at), below).start()
+
+            side_copy(block(at), below).start()
+            core_copy(block(at), at).start()
+
+        @pl.when(above < levels)
+        def _():
+            at = above * 2 + side
+            landed(at)
+
+            @pl.when(level > 0)
+            def _():
+                low_copy(block(at), above).start()
+
+            side_copy(block(at), above).start()
+            core_copy(block(at), at).start()
+
+    def from_side(origin):
+        at = origin * 2 + (1 - side)
+        landed(at)
+        core_copy(block(at), at).start()
+
+    from_side(level)
+    for step in range(1, levels):
+        below = level - step
+        above = level + step
+
+        @pl.when(below >= 0)
+        def _():
+            from_side(below)
+
+        @pl.when(above < levels)
+        def _():
+            from_side(above)
+
+    keep.wait()
+    keep_weight.wait()
+    for copy in weight_copies:
+        copy.wait_send()
+    for other in others:
+        remote(
+            weight_ref, weights_ref.at[other], weight_send.at[0], weight_recv.at[other], core_peer
+        ).wait_recv()
+    for origin in range(levels):
+        side_copy(own_ref, origin).wait_send()
+
+        @pl.when((level < levels - 1) & (origin <= level))
+        def _():
+            up_copy(own_ref, origin).wait_send()
+
+        @pl.when((level > 0) & (origin >= level))
+        def _():
+            low_copy(own_ref, origin).wait_send()
+
+    for at in range(count):
+        core_copy(own_ref, at).wait_send()
+        far = rows_ref.at[1 - core, at]
+        remote(far, far, core_sem.at[at], core_recv.at[at], core_peer).wait_recv()
+    swap.wait()
+
+
+def gather_rows(mid_half, weight_rows, down, half_rows):
+    count = lax.axis_size("sp")
+    levels = count // 2
+    tok_rows, half_width = mid_half.shape
+    vmem = pl.BlockSpec(memory_space=pltpu.VMEM)
+    hbm = pl.BlockSpec(memory_space=pltpu.HBM)
+    dma = pltpu.SemaphoreType.DMA
+    return pl.pallas_call(
+        functools.partial(gather_kernel, levels),
+        out_shape=(
+            jax.ShapeDtypeStruct((2, count, tok_rows, half_width), mid_half.dtype),
+            jax.ShapeDtypeStruct((count,) + weight_rows.shape, weight_rows.dtype),
+            jax.ShapeDtypeStruct((half_rows, down.shape[2]), down.dtype),
+        ),
+        in_specs=[vmem, vmem, hbm],
+        out_specs=(vmem, vmem, hbm),
+        scratch_shapes=[
+            dma((2,)),
+            dma((levels,)),
+            dma((levels,)),
+            dma((levels,)),
+            dma((count,)),
+            dma((count,)),
+            dma((count,)),
+            dma((count - 1,)),
+            dma((count,)),
+            dma((2,)),
+        ],
+        compiler_params=pltpu.CompilerParams(
+            collective_id=0, has_side_effects=True, vmem_limit_bytes=24 * 1024 * 1024
+        ),
+    )(mid_half, weight_rows, down)
+
+
 def body_dense(
     resid,
     a_val,
@@ -161,9 +371,6 @@
     conv_span = conv_kernel.shape[0]
     channels_all = a_val.shape[1] * tp_count
 
-    other_rows = lax.dynamic_slice_in_dim(exp_down[0], (1 - row) * 2 * part_hidden, 2 * part_hidden, 0)
-    swapped_down = swapped(other_rows, "tp", 2)
-
     gated_in = (a_val.astype(jnp.float32) * jax.nn.sigmoid(a_gate.astype(jnp.float32))).astype(
         jnp.bfloat16
     )
@@ -173,8 +380,6 @@
         jnp.where(routes[:, :, None] == expert_ids[None, None, :], route_weights[:, :, None], 0.0),
         axis=1,
     )
-    weight_all = lax.all_gather(weight_mat, "sp", axis=0, tiled=True)
-    weight_own = lax.dynamic_slice_in_dim(weight_all, lax.axis_index("sp"), 1, 1)
     padded = jnp.concatenate([before, gated_in], axis=0).astype(jnp.float32)
     kernel = conv_kernel.astype(jnp.float32)
     conv_out = jnp.broadcast_to(conv_bias[None, :], gated_in.shape)
@@ -195,11 +400,13 @@
     half_sum = chip_sum.astype(jnp.float32) + swapped(chip_sum, "tp", 2).astype(jnp.float32)
     resid_half = lax.dynamic_slice_in_dim(resid, core * half_width, half_width, 1)
     mid_half = (resid_half.astype(jnp.float32) + half_sum).astype(jnp.bfloat16)
-    mid_all = lax.all_gather(mid_half, "sp", axis=0, tiled=True)
-    mid_peer = swapped(mid_half, "tp", 1)
-    first = jnp.where(core == 0, mid_half, mid_peer)
-    second = jnp.where(core == 0, mid_peer, mid_half)
-    middle = jnp.concatenate([first, second], axis=1)
+    gathered, weights_got, swapped_down = gather_rows(
+        mid_half, weight_mat.T, exp_down, 2 * part_hidden
+    )
+    sp_place = lax.axis_index("sp")
+    weight_own = lax.dynamic_index_in_dim(weights_got, sp_place, 1, False).reshape(-1, 1)
+    own_halves = lax.dynamic_index_in_dim(gathered, sp_place, 1, False)
+    middle = jnp.concatenate([own_halves[0], own_halves[1]], axis=1)
 
     middle_f = middle.astype(jnp.float32)
     inverse = lax.rsqrt(jnp.mean(middle_f * middle_f, axis=1, keepdims=True) + RMS_EPS)
@@ -214,10 +421,10 @@
         preferred_element_type=jnp.float32,
     )
 
-    mid_all_peer = swapped(mid_all, "tp", 1)
-    rows_first = jnp.where(core == 0, mid_all, mid_all_peer)
-    rows_second = jnp.where(core == 0, mid_all_peer, mid_all)
-    rows_f = jnp.concatenate([rows_first, rows_second], axis=1).astype(jnp.float32)
+    all_rows = sp_count * tok_rows
+    rows_f = jnp.concatenate(
+        [gathered[0].reshape(all_rows, half_width), gathered[1].reshape(all_rows, half_width)], axis=1
+    ).astype(jnp.float32)
     rows_inverse = lax.rsqrt(jnp.mean(rows_f * rows_f, axis=1, keepdims=True) + RMS_EPS)
     rows = (rows_f * rows_inverse * ffn_gain[None, :]).astype(jnp.bfloat16)
     gate_part = jnp.dot(rows, exp_gate[0], preferred_element_type=jnp.float32)
@@ -228,11 +435,6 @@
     own_at = tp_place * part_hidden
     peer_at = (tp_place ^ 1) * part_hidden
     stay = lax.dynamic_slice_in_dim
-    out_own = jnp.dot(
-        hidden, stay(exp_down[0], own_at, part_hidden, 0), preferred_element_type=jnp.float32
-    ) + jnp.dot(
-        hidden_peer, stay(exp_down[0], peer_at, part_hidden, 0), preferred_element_type=jnp.float32
-    )
     out_far = jnp.dot(
         hidden, stay(swapped_down, core * part_hidden, part_hidden, 0), preferred_element_type=jnp.float32
     ) + jnp.dot(
@@ -240,10 +442,17 @@
         stay(swapped_down, (1 - core) * part_hidden, part_hidden, 0),
         preferred_element_type=jnp.float32,
     )
-    both = jnp.concatenate([out_own * weight_own, out_far * weight_own], axis=1).astype(jnp.bfloat16)
-    summed = lax.psum_scatter(both, "sp", scatter_dimension=0, tiled=True)
-    far = swapped(summed[:, col_width:], "tp", 2)
-    routed = summed[:, :col_width].astype(jnp.float32) + far.astype(jnp.float32)
+    far = swapped((out_far * weight_own).astype(jnp.bfloat16), "tp", 2)
+    out_own = jnp.dot(
+        hidden, stay(exp_down[0], own_at, part_hidden, 0), preferred_element_type=jnp.float32
+    ) + jnp.dot(
+        hidden_peer, stay(exp_down[0], peer_at, part_hidden, 0), preferred_element_type=jnp.float32
+    )
+    expert_sum = (out_own * weight_own + far.astype(jnp.float32)).astype(jnp.bfloat16)
+    returned = lax.all_to_all(
+        expert_sum.reshape(sp_count, tok_rows, col_width), "sp", split_axis=0, concat_axis=0, tiled=True
+    )
+    routed = jnp.sum(returned.astype(jnp.float32), axis=0)
     return (middle_cols.astype(jnp.float32) + shared + routed).astype(jnp.bfloat16)
 
 
@@ -253,7 +462,12 @@
     local_experts = args[11].shape[0]
     experts_all = local_experts * lax.axis_size("sp")
     capacity = 2 * tok_rows * top_count // experts_all
-    if local_experts == 1 and lax.axis_size("tp") == 4 and capacity >= tok_rows:
+    if (
+        local_experts == 1
+        and lax.axis_size("tp") == 4
+        and lax.axis_size("sp") % 2 == 0
+        and capacity >= tok_rows
+    ):
         return body_dense(*args)
     return body_slots(*args)
 

time: 231 us -> 161 us (0.70)
  waiting for transfers between devices: 123 us -> 45.3 us
  Pallas kernels: 0 us -> 51 us
  blocking collectives: 42.6 us -> 11.8 us
  between operations: 13.7 us -> 0.25 us
  other arithmetic: 10.3 us -> 5.25 us
  local copies, waits for them, and re-layouts: 5.9 us -> 8.6 us
  matrix products: 25.8 us -> 28.2 us
    reduce_scatter x1 -> x0, waiting for transfers between devices: 58 us -> none  [body_dense(): summed = lax.psum_scatter(both, 'sp', scatter_dimension=0, tiled=True)]
    pallas_call x0 -> x1, Pallas kernels: none -> 51 us  [gather_rows(): pl.pallas_call(functools.partial(gather_kernel, levels), out_shape=(jax.S...]
    all_gather x1 -> x0, waiting for transfers between devices: 50.1 us -> none  [body_dense(): mid_all = lax.all_gather(mid_half, 'sp', axis=0, tiled=True)]
    all_gather x1 -> x0, blocking collectives: 30.8 us -> none  [body_dense(): weight_all = lax.all_gather(weight_mat, 'sp', axis=0, tiled=True)]
    all_to_all x0 -> x1, waiting for transfers between devices: none -> 16 us  [body_dense(): lax.all_to_all(expert_sum.reshape(sp_count, tok_rows, col_width), 'sp', s...]
    ppermute x7 -> x4, waiting for transfers between devices: 14.8 us -> 29.4 us  [swapped(): return lax.ppermute(value, axis, [(i, i ^ bit) for i in range(size)])]
    all_to_all x0 -> x1, starting transfers between devices: none -> 3.69 us  [body_dense(): lax.all_to_all(expert_sum.reshape(sp_count, tok_rows, col_width), 'sp', s...]
    unnamed x24, local copies, waits for them, and re-layouts: 1.23 us -> 4.89 us
  transfers between devices with their start and end apart: 10 -> 6, of which waited for: 7 -> 5; matrix products, arithmetic and copies ran while one was open for 10% -> 9% of each run, Pallas kernels for 0% -> 0%
where the time goes in v2:
time: 161 us
  Pallas kernels  51 us (32%)
  waiting for transfers between devices  45.3 us (28%)
  matrix products  28.2 us (18%)
  blocking collectives  11.8 us (7%)
  starting transfers between devices  10.1 us (6%)
  local copies, waits for them, and re-layouts  8.6 us (5%)
  other arithmetic  5.25 us (3%)
    pallas_call x1, Pallas kernels, gather_rows(): pl.pallas_call(functools.partial(gather_kernel, levels), out_shape=(jax.S...  51 us
    ppermute x4, waiting for transfers between devices, swapped(): return lax.ppermute(value, axis, [(i, i ^ bit) for i in range(size)])  29.4 us
    all_to_all x1, waiting for transfers between devices, body_dense(): lax.all_to_all(expert_sum.reshape(sp_count, tok_rows, col_width), 'sp', s...  16 us
    dot_general x1, matrix products, body_dense(): gate_part = jnp.dot(rows, exp_gate[0], preferred_element_type=jnp.float32)  6.63 us
    psum x1, blocking collectives, body_dense(): lax.psum((jnp.sum(conv_out, axis=1), jnp.sum(conv_out * conv_out, axis=1)...  6.33 us
    all_gather x1, blocking collectives, body_dense(): lax.all_gather(shared_hidden, 'tp', axis=1, tiled=True)  5.45 us
    unnamed x24, local copies, waits for them, and re-layouts  4.89 us
    ppermute x1, starting transfers between devices, shifted(): return lax.ppermute(value, axis, pairs)  4.88 us
  transfers between devices with their start and end apart: 6, of which 5 were waited for; matrix products, arithmetic and copies ran while one was open for 9% of the time, Pallas kernels for 0%

profile of v2, /device:TPU:0, one launch (start us, length us, event | category | flops | bytes accessed | tf_op | source)
XLA Modules:
  0.0 160.5 jit_solution(16360836745069250348)
XLA Ops:
  1.0 4.9 %collective-permute-start = (bf16[30,256]{1,0:T(8,128)(2,1)S(1)}, bf16[30,256]{1,0:T(8,128)(2,1)S(1)}, u32[]{:S(2)}, u32[]{:S(2)}) collective-permute-start(bf16[30,256]{1,0:T(8,128)(2,1)S(1)} %slice.271), channel_id=1, source_target_pairs={{0,4},{4,8},{8,12},{12,16},{16,20},{20,24},{24,28},{1,5},{5,9},{9,... | collective-permute-start | bytes 46088 | tf_op jit(solution)/shard_map/ppermute | solution.py:17
  8.0 1.3 fusion.72
  9.3 6.3 %all-reduce = (f32[128]{0:T(128)S(1)}, f32[128]{0:T(128)S(1)}) all-reduce(f32[128]{0:T(128)S(1)} %get-tuple-element.12, f32[128]{0:T(128)S(1)} %get-tuple-element.11), channel_id=1, replica_groups=mesh['sp'=8,'tp'=4] {'tp'}, use_global_device_ids=true, to_apply=%region_3.4 | all-reduce | flops 256 | bytes 2048 | tf_op jit(solution)/shard_map/psum | solution.py:388
  16.2 1.5 collective-permute-done.1
  17.8 1.1 collective-permute-start.2
  18.9 7.3 %collective-permute-done.2 = bf16[128,1024]{1,0:T(8,128)(2,1)S(1)} collective-permute-done((bf16[128,1024]{1,0:T(8,128)(2,1)S(1)}, bf16[128,1024]{1,0:T(8,128)(2,1)S(1)}, u32[]{:S(2)}, u32[]{:S(2)}) %collective-permute-start.2) | collective-permute-done | bytes 262176 | tf_op jit(solution)/shard_map/ppermute | solution.py:134
  26.4 2.2 %copy-done.2 = bf16[1,4096,512]{2,1,0:T(8,128)(2,1)S(1)} copy-done((bf16[1,4096,512]{2,1,0:T(8,128)(2,1)S(1)}, bf16[1,4096,512]{2,1,0:T(8,128)(2,1)}, u32[]{:S(2)}) %copy-start.2) | copy-done | bytes 4194328
  28.5 51.0 %shard_map.163 = (bf16[2,8,128,1024]{3,2,1,0:T(8,128)(2,1)S(1)}, f32[8,8,128]{2,1,0:T(8,128)S(1)}, bf16[2048,512]{1,0:T(8,128)(2,1)S(1)}) custom-call(bf16[128,1024]{1,0:T(8,128)(2,1)S(1)} %add_convert_fusion.1.own_ref, f32[8,128]{1,0:T(8,128)S(1)} %bitcast.63, bf16[1,4096,512]{2,1,0:T(8,128)(2,1)S(1)} %copy-done.2), custom_call_target="tpu_custom_call" | custom-call | tf_op jit(solution)/shard_map/pallas_call | solution.py:316
  80.1 1.5 copy-done.1
  82.6 1.2 copy-done.9
  83.8 4.6 %fusion.3 = f32[1024,1024]{1,0:T(8,128)S(1)} fusion(bf16[1,2048,1024]{2,1,0:T(8,128)(2,1)S(1)} %copy-done.9, f32[2048]{0:T(1024)S(1)} %copy-done.11, f32[1024]{0:T(1024)S(1)} %add_rsqrt_fusion, bf16[1024,1024]{1,0:T(8,128)(2,1)S(1)} %bitcast.68, bf16[1024,1024]{1,0:T(8,128)(2,1)S(1)} %bitcast.65), kind=kOutput, calls=%fused_computation.6 | convolution fusion | flops 4309647360 | bytes 12595200 | tf_op jit(solution)/shard_map/dot_general | solution.py:431
  88.4 6.6 %multiply_convert_fusion = bf16[1024,1024]{1,0:T(8,128)(2,1)} fusion(f32[1024,1024]{1,0:T(8,128)S(1)} %fusion.3, bf16[1,2048,1024]{2,1,0:T(8,128)(2,1)S(1)} %copy-done.10, f32[2048]{0:T(1024)S(1)} %copy-done.11, f32[1024]{0:T(1024)S(1)} %add_rsqrt_fusion, bf16[1024,1024]{1,0:T(8,128)(2,1)S(1)} %bitcast.69, bf16[1024,1024]{1,0:T(8,128)(2,1)S(1)} %bitcast.66), kind=kOutput, calls=%fused_computation.10 | convolution fusion | flops 4315938816 | bytes 14692352 | tf_op jit(solution)/shard_map/dot_general | solution.py:430
  95.0 2.8 %fusion.20 = f32[1024,512]{1,0:T(8,128)S(1)} fusion(bf16[1024,1024]{1,0:T(8,128)(2,1)} %multiply_convert_fusion, bf16[2048,512]{1,0:T(8,128)(2,1)S(1)} %get-tuple-element.10, s32[]{:T(128)S(6)} %select_n.36), kind=kOutput, calls=%fused_computation.29 | convolution fusion | flops 1073741824 | bytes 5242884 | tf_op jit(solution)/shard_map/dot_general | solution.py:438
  97.9 1.6 %collective-permute-done.3 = bf16[1024,1024]{1,0:T(8,128)(2,1)} collective-permute-done((bf16[1024,1024]{1,0:T(8,128)(2,1)}, bf16[1024,1024]{1,0:T(8,128)(2,1)}, u32[]{:S(2)}, u32[]{:S(2)}) %collective-permute-start.3) | collective-permute-done | bytes 2097184 | tf_op jit(solution)/shard_map/ppermute | solution.py:134
  99.5 3.9 %multiply_convert_fusion.1 = bf16[1024,512]{1,0:T(8,128)(2,1)} fusion(f32[1024,512]{1,0:T(8,128)S(1)} %fusion.20, bf16[1024,1024]{1,0:T(8,128)(2,1)} %collective-permute-done.3, bf16[2048,512]{1,0:T(8,128)(2,1)S(1)} %get-tuple-element.10, s32[]{:T(128)S(6)} %select_n.37, f32[1024]{0:T(1024)S(1)} %bitcast.70), kind=kOutput, calls=%fused_computation.13 | convolution fusion | flops 1075314688 | bytes 6295556 | tf_op jit(solution)/shard_map/dot_general | solution.py:440
  103.7 3.1 %fusion.17 = f32[1024,512]{1,0:T(8,128)S(1)} fusion(bf16[1024,1024]{1,0:T(8,128)(2,1)} %multiply_convert_fusion, bf16[1,4096,512]{2,1,0:T(8,128)(2,1)} %down_ref.1, s32[]{:T(128)S(6)} %select_n.41), kind=kOutput, calls=%fused_computation.26 | convolution fusion | flops 1073741824 | bytes 5242884 | tf_op jit(solution)/shard_map/dot_general | solution.py:446
  106.8 3.1 %fusion.15 = f32[1024,512]{1,0:T(8,128)S(1)} fusion(bf16[1024,1024]{1,0:T(8,128)(2,1)} %collective-permute-done.3, bf16[1,4096,512]{2,1,0:T(8,128)(2,1)} %down_ref.1, s32[]{:T(128)S(6)} %select_n.42), kind=kOutput, calls=%fused_computation.24 | convolution fusion | flops 1073741824 | bytes 5242884 | tf_op jit(solution)/shard_map/dot_general | solution.py:448
  109.9 18.9 %collective-permute-done.4 = bf16[1024,512]{1,0:T(8,128)(2,1)S(1)} collective-permute-done((bf16[1024,512]{1,0:T(8,128)(2,1)}, bf16[1024,512]{1,0:T(8,128)(2,1)S(1)}, u32[]{:S(2)}, u32[]{:S(2)}) %collective-permute-start.4) | collective-permute-done | bytes 1048608 | tf_op jit(solution)/shard_map/ppermute | solution.py:134
  128.8 1.4 add_convert_fusion
  130.2 3.7 %all-to-all-start = ((bf16[8,128,512]{2,1,0:T(8,128)(2,1)}), bf16[8,128,512]{2,1,0:T(8,128)(2,1)S(1)}, u32[]{:S(2)}, u32[]{:S(2)}) async-start(bf16[8,128,512]{2,1,0:T(8,128)(2,1)} %bitcast.41), calls=%async_computation | async-start | bytes 2097152 | tf_op jit(solution)/shard_map/all_to_all | solution.py:452
  135.2 1.4 fusion.68
  136.6 1.4 fusion.11
  138.0 5.4 %all_gather.3 = bf16[128,512]{1,0:T(8,128)(2,1)S(1)} all-gather(bf16[128,128]{1,0:T(8,128)(2,1)S(1)} %fusion.11), channel_id=1, replica_groups=mesh['sp'=8,'tp'=4] {'tp'}, dimensions={1}, use_global_device_ids=true | all-gather | bytes 163840 | tf_op jit(solution)/shard_map/all_gather | solution.py:419
  143.5 16.0 %all-to-all-done = bf16[8,128,512]{2,1,0:T(8,128)(2,1)S(1)} async-done(((bf16[8,128,512]{2,1,0:T(8,128)(2,1)}), bf16[8,128,512]{2,1,0:T(8,128)(2,1)S(1)}, u32[]{:S(2)}, u32[]{:S(2)}) %all-to-all-start) | async-done | bytes 1048608 | tf_op jit(solution)/shard_map/all_to_all | solution.py:452
  (45 shorter events, 7.9 us)
Async XLA Ops:
  0.0 15.7 %copy-start = (bf16[256,2048]{1,0:T(8,128)(2,1)S(1)}, bf16[256,2048]{1,0:T(8,128)(2,1)}, u32[]{:S(2)}) copy-start(bf16[256,2048]{1,0:T(8,128)(2,1)} %param.24) | copy-start | bytes 3145732
  0.0 15.7 %copy-start.7 = (f32[256]{0:T(256)S(1)}, f32[256]{0:T(256)}, u32[]{:S(2)}) copy-start(f32[256]{0:T(256)} %param.23) | copy-start | bytes 3076
  0.0 15.7 %copy-start.8 = (f32[256]{0:T(256)S(1)}, f32[256]{0:T(256)}, u32[]{:S(2)}) copy-start(f32[256]{0:T(256)} %param.22) | copy-start | bytes 3076
  1.0 6.9 %collective-permute-start = (bf16[30,256]{1,0:T(8,128)(2,1)S(1)}, bf16[30,256]{1,0:T(8,128)(2,1)S(1)}, u32[]{:S(2)}, u32[]{:S(2)}) collective-permute-start(bf16[30,256]{1,0:T(8,128)(2,1)S(1)} %slice.271), channel_id=1, source_target_pairs={{0,4},{4,8},{8,12},{12,16},{16,20},{20,24},{24,28},{1,5},{5,9},{9,... | collective-permute-start | bytes 46088 | tf_op jit(solution)/shard_map/ppermute | solution.py:17
  7.9 11.0 %copy-start.5 = (f32[128,4]{0,1:T(4,128)S(1)}, f32[128,4]{0,1:T(4,128)}, u32[]{:S(2)}) copy-start(f32[128,4]{0,1:T(4,128)} %param.27) | copy-start | bytes 6148
  7.9 11.0 %copy-start.6 = (s32[128,4]{0,1:T(4,128)S(1)}, s32[128,4]{0,1:T(4,128)}, u32[]{:S(2)}) copy-start(s32[128,4]{0,1:T(4,128)} %param.26) | copy-start | bytes 6148
  7.9 18.3 %copy-start.4 = (bf16[128,2048]{1,0:T(8,128)(2,1)S(1)}, bf16[128,2048]{1,0:T(8,128)(2,1)}, u32[]{:S(2)}) copy-start(bf16[128,2048]{1,0:T(8,128)(2,1)} %param.17) | copy-start | bytes 1572868
  16.1 1.6 collective-permute-start.1
  17.8 8.4 %collective-permute-start.2 = (bf16[128,1024]{1,0:T(8,128)(2,1)S(1)}, bf16[128,1024]{1,0:T(8,128)(2,1)S(1)}, u32[]{:S(2)}, u32[]{:S(2)}) collective-permute-start(bf16[128,1024]{1,0:T(8,128)(2,1)S(1)} %add_convert_fusion.2), channel_id=1, source_target_pairs={{0,2},{1,3},{2,0},{3,1},{4,6},{5,7},{6,4},{7,5},{8,10},{9,11},{10,... | collective-permute-start | bytes 786440 | tf_op jit(solution)/shard_map/ppermute | solution.py:134
  26.3 2.2 %copy-start.2 = (bf16[1,4096,512]{2,1,0:T(8,128)(2,1)S(1)}, bf16[1,4096,512]{2,1,0:T(8,128)(2,1)}, u32[]{:S(2)}) copy-start(bf16[1,4096,512]{2,1,0:T(8,128)(2,1)} %down_ref.1) | copy-start | bytes 12582916
  79.5 2.1 %copy-start.1 = (bf16[2,8,128,1024]{3,2,1,0:T(8,128)(2,1)}, bf16[2,8,128,1024]{3,2,1,0:T(8,128)(2,1)S(1)}, u32[]{:S(2)}) copy-start(bf16[2,8,128,1024]{3,2,1,0:T(8,128)(2,1)S(1)} %get-tuple-element.8) | copy-start | bytes 12582916
  81.6 2.2 %copy-start.9 = (bf16[1,2048,1024]{2,1,0:T(8,128)(2,1)S(1)}, bf16[1,2048,1024]{2,1,0:T(8,128)(2,1)}, u32[]{:S(2)}) copy-start(bf16[1,2048,1024]{2,1,0:T(8,128)(2,1)} %param.29) | copy-start | bytes 12582916
  81.6 2.2 %copy-start.11 = (f32[2048]{0:T(1024)S(1)}, f32[2048]{0:T(1024)}, u32[]{:S(2)}) copy-start(f32[2048]{0:T(1024)} %param.25) | copy-start | bytes 24580
  83.8 4.6 %copy-start.10 = (bf16[1,2048,1024]{2,1,0:T(8,128)(2,1)S(1)}, bf16[1,2048,1024]{2,1,0:T(8,128)(2,1)}, u32[]{:S(2)}) copy-start(bf16[1,2048,1024]{2,1,0:T(8,128)(2,1)} %param.28) | copy-start | bytes 12582916
  95.0 4.5 %collective-permute-start.3 = (bf16[1024,1024]{1,0:T(8,128)(2,1)}, bf16[1024,1024]{1,0:T(8,128)(2,1)}, u32[]{:S(2)}, u32[]{:S(2)}) collective-permute-start(bf16[1024,1024]{1,0:T(8,128)(2,1)} %multiply_convert_fusion), channel_id=1, source_target_pairs={{0,1},{1,0},{2,3},{3,2},{4,5},{5,4},{6,7},{7,6},{8,9},{9,8},{10,11... | collective-permute-start | bytes 6291464 | tf_op jit(solution)/shard_map/ppermute | solution.py:134
  103.4 25.4 %collective-permute-start.4 = (bf16[1024,512]{1,0:T(8,128)(2,1)}, bf16[1024,512]{1,0:T(8,128)(2,1)S(1)}, u32[]{:S(2)}, u32[]{:S(2)}) collective-permute-start(bf16[1024,512]{1,0:T(8,128)(2,1)} %multiply_convert_fusion.1), channel_id=1, source_target_pairs={{0,2},{1,3},{2,0},{3,1},{4,6},{5,7},{6,4},{7,5},{8,10},{9,11},{10,... | collective-permute-start | bytes 3145736 | tf_op jit(solution)/shard_map/ppermute | solution.py:134
  130.2 29.4 %copy-start.3 = (bf16[512,512]{1,0:T(8,128)(2,1)S(1)}, bf16[512,512]{1,0:T(8,128)(2,1)}, u32[]{:S(2)}) copy-start(bf16[512,512]{1,0:T(8,128)(2,1)} %param.33) | copy-start | bytes 1572868
  130.2 29.2 %all-to-all-start = ((bf16[8,128,512]{2,1,0:T(8,128)(2,1)}), bf16[8,128,512]{2,1,0:T(8,128)(2,1)S(1)}, u32[]{:S(2)}, u32[]{:S(2)}) async-start(bf16[8,128,512]{2,1,0:T(8,128)(2,1)} %bitcast.41), calls=%async_computation | async-start | bytes 2097152 | tf_op jit(solution)/shard_map/all_to_all | solution.py:452
